TPU v7x, 1024 devices: a whole 4x8x16 slice. The times are simulated.
1024 devices in a mesh: ep: 32 (over z, core), tp: 32 (over y, x).
Axes of the slice: x: 4, y: 8, z: 16, core: 2. Of those that a mesh axis runs over, the one named last changes fastest.
Arguments:
- tokens: bfloat16 [4096, 2048], P('ep'), may hold values from -6 to 6
- cotangent: bfloat16 [4096, 2048], P('ep'), may hold values from -6 to 6
- routes: int32 [4096, 2], P('ep'), may hold values from 0 to 31, all different within a row; in each aligned block of 128 rows (0 to 127, 128 to 255, ...) at most 16 rows name the same one
- route_weight: float32 [4096, 2], P('ep'), may hold values from 0.1 to 1
- w_gate: bfloat16 [32, 2048, 1024], P('ep', None, 'tp'), may hold values from -0.25 to 0.25
- w_up: bfloat16 [32, 2048, 1024], P('ep', None, 'tp'), may hold values from -0.25 to 0.25
- w_down: bfloat16 [32, 1024, 2048], P('ep', 'tp'), may hold values from -0.1875 to 0.1875
Outputs:
- grad_tokens: bfloat16 [4096, 2048], P('ep', 'tp')
- grad_route_weight: float32 [4096, 2], P('ep')
- grad_gate: float32 [32, 2048, 1024], P('ep', None, 'tp')
- grad_up: float32 [32, 2048, 1024], P('ep', None, 'tp')
- grad_down: float32 [32, 1024, 2048], P('ep', 'tp')
Inputs may be any that keep to these rules, and one draw needn't show every extreme that they name: `routes`: each row names 2 different experts. In each aligned block of 128 rows (the rows of one index of ep) no expert is named by more than 16 rows, and in every draw some expert is named by exactly 16 rows of some block.
All inputs are finite; a program needn't handle non-finite values.
Results may differ from a plain program's by a relative error of at most 0.023.
Values may be sent and summed in bfloat16 or wider, within the bound.
A program may use at most 32 MiB of HBM per device.

v0:
```python
import jax
import jax.numpy as jnp
from jax import lax
from jax.sharding import PartitionSpec as P


def rows_first(arrays, axis, dims):
    turned = [jnp.moveaxis(a, dim, 0) for a, dim in zip(arrays, dims)]
    both = jnp.concatenate([t.reshape(len(t), -1) for t in turned], axis=1)
    whole, at, finished = (lax.all_gather(both, axis, axis=0, tiled=True), 0, [])
    for t, dim in zip(turned, dims):
        share = whole[:, at : at + t[0].size].reshape(-1, *t.shape[1:])
        finished.append(jnp.moveaxis(share, 0, dim))
        at += t[0].size
    return tuple(finished)


def in_blocks(value, dim, length):
    dims = value.shape
    parts = value.reshape(*dims[:dim], length, dims[dim] // length, *dims[dim + 1 :])
    return jnp.moveaxis(parts, dim, 0)


def summed_on_arrival(value, axis, dim):
    length = lax.axis_size(axis)
    parts = lax.all_to_all(in_blocks(value, dim, length), axis, 0, 0, tiled=True)
    return jnp.sum(parts.astype(jnp.float32), axis=0)


def sent_to_all(value, axis):
    length = lax.axis_size(axis)
    return lax.all_to_all(
        jnp.broadcast_to(value[None], (length, *value.shape)), axis, 0, 0, tiled=True
    )


def taken_together(value, axis):
    return sent_to_all(value, axis).sum(axis=0)


def slot_index(block_routes, experts, capacity):
    flat_ids = block_routes.reshape(-1)
    onehot = (flat_ids[:, None] == jnp.arange(experts, dtype=jnp.int32)[None, :]).astype(jnp.int32)
    earlier = jnp.cumsum(onehot, axis=0) - onehot
    return flat_ids * capacity + jnp.sum(earlier * onehot, axis=1)


def on_device(tokens, cotangent, routes, route_weight, w_gate, w_up, w_down):
    f32 = jnp.float32
    tok_rows, model_width = tokens.shape
    choices_row = routes.shape[1]
    experts = lax.axis_size("ep")
    capacity = 2 * tok_rows * choices_row // experts
    recv_rows = experts * capacity
    slot_ids = slot_index(routes, experts, capacity)
    send_w = jnp.zeros((recv_rows,), f32).at[slot_ids].set(route_weight.reshape(-1))
    share = model_width // lax.axis_size("tp")
    offset = lax.axis_index("tp") * share
    tok_share = lax.dynamic_slice_in_dim(tokens, offset, share, 1)
    cot_share = lax.dynamic_slice_in_dim(cotangent, offset, share, 1)
    send_x = (
        jnp.zeros((recv_rows, share), jnp.bfloat16)
        .at[slot_ids]
        .set(jnp.repeat(tok_share, choices_row, axis=0))
    )
    send_dy = (
        jnp.zeros((recv_rows, share), jnp.bfloat16)
        .at[slot_ids]
        .set(jnp.repeat(cot_share, choices_row, axis=0))
    )
    part_x, part_dy, got_w = (
        lax.all_to_all(
            send_x.reshape(experts, capacity, share), "ep", split_axis=0, concat_axis=0, tiled=True
        ),
        lax.all_to_all(
            send_dy.reshape(experts, capacity, share), "ep", split_axis=0, concat_axis=0, tiled=True
        ),
        lax.all_to_all(
            send_w.reshape(experts, capacity, 1).astype(jnp.bfloat16),
            "ep",
            split_axis=0,
            concat_axis=0,
            tiled=True,
        ).astype(jnp.float32),
    )
    got_x, got_dy = rows_first((part_x, part_dy), "tp", (2, 2))
    rows_x = got_x.reshape(recv_rows, model_width)
    rows_dy = got_dy.reshape(recv_rows, model_width)
    rows_w = got_w.reshape(recv_rows)
    gate_w = w_gate[0]
    up_w = w_up[0]
    down_w = w_down[0]
    gate_pre = jnp.dot(rows_x, gate_w, preferred_element_type=f32)
    up_pre = jnp.dot(rows_x, up_w, preferred_element_type=f32)
    gate_sig = jax.nn.sigmoid(gate_pre)
    act_full = gate_pre * gate_sig * up_pre
    act = act_full.astype(jnp.bfloat16)
    back_hidden = jnp.einsum("rd,fd->rf", rows_dy, down_w, preferred_element_type=f32)
    weighted_cot = (rows_w[:, None] * rows_dy.astype(f32)).astype(jnp.bfloat16)
    d_hidden = rows_w[:, None] * back_hidden
    d_gate = (d_hidden * up_pre * gate_sig * (1.0 + gate_pre * (1.0 - gate_sig))).astype(
        jnp.bfloat16
    )
    d_up = (d_hidden * gate_pre * gate_sig).astype(jnp.bfloat16)
    gate_part = jnp.sum(act_full * back_hidden, axis=1)
    token_part = jnp.einsum("rf,df->rd", d_gate, gate_w, preferred_element_type=f32)
    token_part = token_part + jnp.einsum("rf,df->rd", d_up, up_w, preferred_element_type=f32)
    grad_gate = jnp.einsum("rd,rf->df", rows_x, d_gate, preferred_element_type=f32)[None]
    grad_up = jnp.einsum("rd,rf->df", rows_x, d_up, preferred_element_type=f32)[None]
    grad_down = jnp.einsum("rf,rd->fd", act, weighted_cot, preferred_element_type=f32)[None]
    rounded_part = token_part.astype(jnp.bfloat16).astype(f32)
    shares = summed_on_arrival(rounded_part.astype(jnp.bfloat16), "tp", 1)
    gate_total = taken_together(gate_part, "tp")
    route_grad = shares.astype(jnp.bfloat16)
    back_x, back_gate = (
        lax.all_to_all(
            route_grad.reshape(experts, capacity, -1), "ep", split_axis=0, concat_axis=0, tiled=True
        ),
        lax.all_to_all(
            gate_total.reshape(experts, capacity).astype(jnp.bfloat16),
            "ep",
            split_axis=0,
            concat_axis=0,
            tiled=True,
        ).astype(jnp.float32),
    )
    picked = back_x.reshape(recv_rows, -1)[slot_ids].astype(f32).reshape(tok_rows, choices_row, -1)
    grad_route_weight = back_gate.reshape(recv_rows)[slot_ids].reshape(tok_rows, choices_row)
    grad_tokens = jnp.sum(picked, axis=1).astype(jnp.bfloat16)
    return (grad_tokens, grad_route_weight, grad_gate, grad_up, grad_down)


def solution(mesh):
    return jax.shard_map(
        on_device,
        mesh=mesh,
        in_specs=(
            P("ep", None),
            P("ep", None),
            P("ep", None),
            P("ep", None),
            P("ep", None, "tp"),
            P("ep", None, "tp"),
            P("ep", "tp", None),
        ),
        out_specs=(
            P("ep", "tp"),
            P("ep", None),
            P("ep", None, "tp"),
            P("ep", None, "tp"),
            P("ep", "tp", None),
        ),
        check_vma=False,
    )
```

profile of v0, /device:TPU:1, one launch (start us, length us, event | category | flops | bytes accessed | tf_op | source)
XLA Modules:
  0.0 288.8 jit_solution(14239841174754783946)
XLA Ops:
  7.2 0.7 broadcast_multiply_fusion
  7.9 0.8 copy.61
  8.7 0.1 eq.29
  8.8 0.1 eq.25
  9.0 0.1 copy.60
  9.1 0.1 mul.72
  9.3 0.6 reduce-window.6
  9.8 0.2 slice_reduce_fusion
  10.1 0.1 fusion.22
  10.2 0.9 constant_dynamic-slice_fusion
  11.1 1.2 scatter_custom_fusion.2
  12.3 0.8 reshape.219
  13.1 20.4 %all-to-all-start.2 = ((bf16[32,2,512]{2,1,0:T(2,128)(2,1)}), bf16[32,2,512]{2,1,0:T(2,128)(2,1)S(1)}, u32[]{:S(2)}, u32[]{:S(2)}) async-start(bf16[32,2,512]{2,1,0:T(2,128)(2,1)} %reshape.219), calls=%async_computation.2 | async-start | bytes 131072 | tf_op jit(solution)/shard_map/all_to_all | solution.py:75
  33.6 1.2 scatter_custom_fusion.1
  34.8 0.8 reshape.221
  35.5 11.0 %all-to-all-done.2 = bf16[32,2,512]{2,1,0:T(2,128)(2,1)S(1)} async-done(((bf16[32,2,512]{2,1,0:T(2,128)(2,1)}), bf16[32,2,512]{2,1,0:T(2,128)(2,1)S(1)}, u32[]{:S(2)}, u32[]{:S(2)}) %all-to-all-start.2) | async-done | bytes 65568 | tf_op jit(solution)/shard_map/all_to_all | solution.py:75
  46.5 5.1 %all-to-all-start.1 = ((bf16[32,2,512]{2,1,0:T(2,128)(2,1)}), bf16[32,2,512]{2,1,0:T(2,128)(2,1)S(1)}, u32[]{:S(2)}, u32[]{:S(2)}) async-start(bf16[32,2,512]{2,1,0:T(2,128)(2,1)} %reshape.221), calls=%async_computation.1 | async-start | bytes 131072 | tf_op jit(solution)/shard_map/all_to_all | solution.py:72
  51.7 0.1 reshape.220
  51.8 12.8 %all-to-all-done.1 = bf16[32,2,512]{2,1,0:T(2,128)(2,1)S(1)} async-done(((bf16[32,2,512]{2,1,0:T(2,128)(2,1)}), bf16[32,2,512]{2,1,0:T(2,128)(2,1)S(1)}, u32[]{:S(2)}, u32[]{:S(2)}) %all-to-all-start.1) | async-done | bytes 65568 | tf_op jit(solution)/shard_map/all_to_all | solution.py:72
  64.7 0.1 reshape.222
  64.8 0.1 pad_maximum_fusion
  64.9 0.8 copy.66
  65.7 0.1 copy.64
  65.8 0.1 reshape.180
  65.9 1.4 scatter_custom_fusion
  67.4 0.1 convert_element_type.82
  67.5 16.2 %all_to_all.37 = bf16[32,16,1]{1,2,0:T(2,128)(2,1)S(1)} all-to-all(bf16[32,16,1]{1,2,0:T(2,128)(2,1)S(1)} %convert_element_type.82), channel_id=1, replica_groups=mesh['ep'=32,'tp'=32] {'ep'}, dimensions={0} | all-to-all | bytes 2048 | tf_op jit(solution)/shard_map/all_to_all | solution.py:78
  83.7 0.1 reshape.158
  83.8 68.4 %all-gather.2.cloned.1.call-done = bf16[2048,1024]{1,0:T(8,128)(2,1)} async-done(((bf16[64,1024]{1,0:T(8,128)(2,1)}), bf16[2048,1024]{1,0:T(8,128)(2,1)}) %all-gather.2.cloned.1.call-update) | async-done | bytes 4194320 | tf_op jit(solution)/shard_map/all_gather | solution.py:10
  152.2 3.8 %fusion.27 = (bf16[2048,512]{1,0:T(8,128)(2,1)S(1)}, bf16[2048,512]{1,0:T(8,128)(2,1)}) fusion(bf16[2048,1024]{1,0:T(8,128)(2,1)} %all-gather.2.cloned.1.call-done), kind=kLoop, calls=%fused_computation.55 | loop fusion | bytes 8388608 | tf_op jit(solution)/shard_map/slice | solution.py:12
  156.0 2.5 copy.77
  158.4 2.9 %copy.76 = bf16[2048,512]{0,1:T(8,128)(2,1)S(1)} copy(bf16[2048,512]{1,0:T(8,128)(2,1)} %get-tuple-element.31) | data formatting | bytes 4194304
  161.4 0.7 fusion.5
  162.1 0.1 copy-done.2
  162.3 0.7 fusion.7
  163.1 0.8 multiply_reduce_fusion
  163.8 0.7 broadcast_in_dim.33
  164.5 6.1 %all-to-all-start.5 = ((f32[32,1,512]{2,1,0:T(1,128)}), f32[32,1,512]{2,1,0:T(1,128)S(1)}, u32[]{:S(2)}, u32[]{:S(2)}) async-start(f32[32,1,512]{2,1,0:T(1,128)} %broadcast_in_dim.33), calls=%async_computation.5 | async-start | bytes 131072 | tf_op jit(solution)/shard_map/all_to_all | solution.py:32
  170.6 0.7 fusion.10
  171.3 2.1 add_convert_fusion
  173.4 3.9 %copy.69 = bf16[512,2048]{0,1:T(8,128)(2,1)} copy(bf16[512,2048]{1,0:T(8,128)(2,1)} %add_convert_fusion) | data formatting | bytes 4194304 | tf_op jit(solution)/shard_map/convert_element_type | solution.py:111
  177.3 2.1 all-to-all-done.5
  179.4 7.2 %all-to-all-start.3 = ((bf16[32,512,64]{1,2,0:T(8,128)(2,1)}), bf16[32,512,64]{1,2,0:T(8,128)(2,1)}, u32[]{:S(2)}, u32[]{:S(2)}) async-start(bf16[32,512,64]{1,2,0:T(8,128)(2,1)} %bitcast.91), calls=%async_computation.3 | async-start | bytes 4194304 | tf_op jit(solution)/shard_map/all_to_all | solution.py:26
  186.7 2.9 %convolution_bitcast_fusion.2 = f32[1,32,2048]{2,1,0:T(8,128)} fusion(bf16[2048,512]{0,1:T(8,128)(2,1)} %copy.77, f32[512]{0:T(512)S(1)} %reshape.158, f32[512,32]{0,1:T(8,128)S(1)} %fusion.7, f32[512,32]{0,1:T(8,128)S(1)} %fusion.5), kind=kOutput, calls=%fused_computation.9 | convolution fusion | flops 70352896 | bytes 2492416 | tf_op jit(solution)/shard_map/rf,rd->fd/dot_general | solution.py:110
  189.6 0.1 reduce_sum.58
  189.7 0.7 convert_element_type.83
  190.4 41.2 %all-to-all-done.3 = bf16[32,512,64]{1,2,0:T(8,128)(2,1)} async-done(((bf16[32,512,64]{1,2,0:T(8,128)(2,1)}), bf16[32,512,64]{1,2,0:T(8,128)(2,1)}, u32[]{:S(2)}, u32[]{:S(2)}) %all-to-all-start.3) | async-done | bytes 2097184 | tf_op jit(solution)/shard_map/all_to_all | solution.py:26
  231.6 19.3 %all-to-all-start.6 = ((bf16[32,1,16]{2,1,0:T(2,128)(2,1)}), bf16[32,1,16]{2,1,0:T(2,128)(2,1)S(1)}, u32[]{:S(2)}, u32[]{:S(2)}) async-start(bf16[32,1,16]{2,1,0:T(2,128)(2,1)} %convert_element_type.83), calls=%async_computation.6 | async-start | bytes 32768 | tf_op jit(solution)/shard_map/all_to_all | solution.py:119
  250.9 1.2 convolution_bitcast_fusion.1
  252.1 1.9 reduce_sum.55
  254.0 0.1 copy.70
  254.1 0.8 reshape.223
  254.8 7.8 %all-to-all-done.6 = bf16[32,1,16]{2,1,0:T(2,128)(2,1)S(1)} async-done(((bf16[32,1,16]{2,1,0:T(2,128)(2,1)}), bf16[32,1,16]{2,1,0:T(2,128)(2,1)S(1)}, u32[]{:S(2)}, u32[]{:S(2)}) %all-to-all-start.6) | async-done | bytes 1056 | tf_op jit(solution)/shard_map/all_to_all | solution.py:119
  262.6 4.4 %all-to-all-start.4 = ((bf16[32,2,512]{2,1,0:T(2,128)(2,1)}), bf16[32,2,512]{2,1,0:T(2,128)(2,1)S(1)}, u32[]{:S(2)}, u32[]{:S(2)}) async-start(bf16[32,2,512]{2,1,0:T(2,128)(2,1)} %reshape.223), calls=%async_computation.4 | async-start | bytes 131072 | tf_op jit(solution)/shard_map/all_to_all | solution.py:116
  267.1 1.2 convolution_bitcast_fusion
  268.3 0.1 reshape.159
  268.4 1.9 gather_fusion.1
  270.3 0.1 reshape.157
  270.5 0.6 copy.74
  271.1 9.0 %all-to-all-done.4 = bf16[32,2,512]{2,1,0:T(2,128)(2,1)S(1)} async-done(((bf16[32,2,512]{2,1,0:T(2,128)(2,1)}), bf16[32,2,512]{2,1,0:T(2,128)(2,1)S(1)}, u32[]{:S(2)}, u32[]{:S(2)}) %all-to-all-start.4) | async-done | bytes 65568 | tf_op jit(solution)/shard_map/all_to_all | solution.py:116
  280.1 0.1 reshape.224
  280.2 0.9 gather_fusion
  281.1 0.2 reduce_sum.56
  281.3 0.7 copy.73
  (21 shorter events, 0.4 us)
Async XLA Ops:
  7.2 154.2 %copy-start = (bf16[1,2048,32]{1,2,0:T(8,128)(2,1)S(1)}, bf16[1,2048,32]{1,2,0:T(8,128)(2,1)}, u32[]{:S(2)}) copy-start(bf16[1,2048,32]{1,2,0:T(8,128)(2,1)} %param.11) | copy-start | bytes 393220
  7.2 58.5 %copy-start.4 = (f32[128,2]{0,1:T(2,128)S(1)}, f32[128,2]{0,1:T(2,128)}, u32[]{:S(2)}) copy-start(f32[128,2]{0,1:T(2,128)} %param.10) | copy-start | bytes 3076
  13.1 33.4 %all-to-all-start.2 = ((bf16[32,2,512]{2,1,0:T(2,128)(2,1)}), bf16[32,2,512]{2,1,0:T(2,128)(2,1)S(1)}, u32[]{:S(2)}, u32[]{:S(2)}) async-start(bf16[32,2,512]{2,1,0:T(2,128)(2,1)} %reshape.219), calls=%async_computation.2 | async-start | bytes 131072 | tf_op jit(solution)/shard_map/all_to_all | solution.py:75
  46.5 18.1 %all-to-all-start.1 = ((bf16[32,2,512]{2,1,0:T(2,128)(2,1)}), bf16[32,2,512]{2,1,0:T(2,128)(2,1)S(1)}, u32[]{:S(2)}, u32[]{:S(2)}) async-start(bf16[32,2,512]{2,1,0:T(2,128)(2,1)} %reshape.221), calls=%async_computation.1 | async-start | bytes 131072 | tf_op jit(solution)/shard_map/all_to_all | solution.py:72
  51.6 100.5 %all-gather.2.cloned.1.call-start = ((), (), s32[]{:S(2)}) async-start(), calls=%async_computation.7 | async-start | bytes 4325376 | tf_op jit(solution)/shard_map/all_gather | solution.py:10
  161.4 0.9 copy-start.2
  161.4 1.7 copy-start.1
  161.4 1.7 copy-start.3
  164.5 14.9 %all-to-all-start.5 = ((f32[32,1,512]{2,1,0:T(1,128)}), f32[32,1,512]{2,1,0:T(1,128)S(1)}, u32[]{:S(2)}, u32[]{:S(2)}) async-start(f32[32,1,512]{2,1,0:T(1,128)} %broadcast_in_dim.33), calls=%async_computation.5 | async-start | bytes 131072 | tf_op jit(solution)/shard_map/all_to_all | solution.py:32
  179.4 52.2 %all-to-all-start.3 = ((bf16[32,512,64]{1,2,0:T(8,128)(2,1)}), bf16[32,512,64]{1,2,0:T(8,128)(2,1)}, u32[]{:S(2)}, u32[]{:S(2)}) async-start(bf16[32,512,64]{1,2,0:T(8,128)(2,1)} %bitcast.91), calls=%async_computation.3 | async-start | bytes 4194304 | tf_op jit(solution)/shard_map/all_to_all | solution.py:26
  231.6 31.0 %all-to-all-start.6 = ((bf16[32,1,16]{2,1,0:T(2,128)(2,1)}), bf16[32,1,16]{2,1,0:T(2,128)(2,1)S(1)}, u32[]{:S(2)}, u32[]{:S(2)}) async-start(bf16[32,1,16]{2,1,0:T(2,128)(2,1)} %convert_element_type.83), calls=%async_computation.6 | async-start | bytes 32768 | tf_op jit(solution)/shard_map/all_to_all | solution.py:119
  262.6 17.4 %all-to-all-start.4 = ((bf16[32,2,512]{2,1,0:T(2,128)(2,1)}), bf16[32,2,512]{2,1,0:T(2,128)(2,1)S(1)}, u32[]{:S(2)}, u32[]{:S(2)}) async-start(bf16[32,2,512]{2,1,0:T(2,128)(2,1)} %reshape.223), calls=%async_computation.4 | async-start | bytes 131072 | tf_op jit(solution)/shard_map/all_to_all | solution.py:116
Sparse Core Ops, SparseCore 0:
  65.8 86.3 all-gather.1
where the time goes:
time: 290 us; the launch traced here: 289 us
  waiting for transfers between devices  152 us (52%)
  starting transfers between devices  62.6 us (22%)
  local copies, waits for them, and re-layouts  29.4 us (10%)
  blocking collectives  16.2 us (6%)
  between operations  14.3 us (5%)
  matrix products  10.2 us (4%)
  other arithmetic  3.77 us (1%)
    all_gather x1, waiting for transfers between devices, rows_first(): lax.all_gather(both, axis, axis=0, tiled=True)  68.4 us
    all_to_all x1, waiting for transfers between devices, summed_on_arrival(): lax.all_to_all(in_blocks(value, dim, length), axis, 0, 0, tiled=True)  41.2 us
    all_to_all x1, starting transfers between devices, on_device(): lax.all_to_all(send_dy.reshape(experts, capacity, share), 'ep', split_axi...  20.4 us
    all_to_all x1, starting transfers between devices, on_device(): lax.all_to_all(gate_total.reshape(experts, capacity).astype(jnp.bfloat16)...  19.3 us
    all_to_all x1, blocking collectives, on_device(): lax.all_to_all(send_w.reshape(experts, capacity, 1).astype(jnp.bfloat16),...  16.2 us
    all_to_all x1, waiting for transfers between devices, on_device(): lax.all_to_all(send_x.reshape(experts, capacity, share), 'ep', split_axis...  12.8 us
    all_to_all x1, waiting for transfers between devices, on_device(): lax.all_to_all(send_dy.reshape(experts, capacity, share), 'ep', split_axi...  11 us
    unnamed x22, local copies, waits for them, and re-layouts  10.5 us
  transfers between devices with their start and end apart: 7, of which 7 were waited for; matrix products, arithmetic and copies ran while one was open for 8% of the time, Pallas kernels for 0%

commit v1 on v0

v1 whole, which is shorter than its diff:
```python
import functools

import jax
import jax.numpy as jnp
from jax import lax
from jax.experimental import pallas as pl
from jax.experimental.pallas import tpu as pltpu
from jax.sharding import PartitionSpec as P

MESH = pl.DeviceIdType.MESH
F32 = jnp.float32
BF16 = jnp.bfloat16
LANES = 128
FEAT = 64
HID = 32
CHUNKS = 4


def dot(a, b, ca, cb):
    return lax.dot_general(a, b, (((ca,), (cb,)), ((), ())), preferred_element_type=F32)


def kernel(
    nz, ny, nx, cap,
    tokens, cotangent, routes, weights, gate_w, up_w, down_w,
    out_tok, out_rw, out_gate, out_up, out_down,
    tok_in, cot_in, gate_in, up_in, down_in,
    onehot0, onehot1, send, rows, w_send, w_all, w_left, w_right,
    part_send, part_got, hidden, piece, piece_got, rw_row, rw_got,
    back, back_got, grad_send, grad_got,
    in_sem, z_send, z_recv, w_ssem, w_rsem, ag_ssem, ag_rsem,
    px_ssem, px_rsem, hx_ssem, hx_rsem, ry_ssem, ry_rsem, rw_ssem, rw_rsem,
    b_ssem, b_rsem, g_ssem, g_rsem,
):
    nep = 2 * nz
    count = nep * cap
    half = count // 2
    tok_dev = tokens.shape[0]
    ep = lax.axis_index("ep")
    tp = lax.axis_index("tp")
    z, core = ep // 2, ep % 2
    y, x = tp // nx, tp % nx

    def remote(src, dst, ssem, rsem, to_ep, to_tp):
        return pltpu.make_async_remote_copy(
            src_ref=src, dst_ref=dst, send_sem=ssem, recv_sem=rsem,
            device_id=(to_ep, to_tp), device_id_type=MESH,
        )

    def arrived(ref, sem):
        pltpu.make_async_copy(ref, ref, sem).wait()

    def ep_peer(i, c):
        k = (i + 1) // 2
        dz = nz // 2 + k - 2 * k * (i % 2)
        return ((z + dz) % nz) * 2 + (core + c) % 2

    def x_peer(d):
        return y * nx + (x + d) % nx

    def y_peer(d):
        return ((y + d) % ny) * nx + x

    def col(i):
        return pl.ds(pl.multiple_of(i * LANES, LANES), LANES)

    def slot(e):
        return pl.ds(pl.multiple_of(e * cap, cap), cap)

    barrier = pltpu.get_barrier_semaphore()

    def greet(to_ep, to_tp):
        pl.semaphore_signal(barrier, inc=1, device_id=(to_ep, to_tp), device_id_type=MESH)

    def greet_ep(i, carry):
        greet(ep_peer(i, 0), tp)
        greet(ep_peer(i, 1), tp)
        return carry

    lax.fori_loop(0, nz - 1, greet_ep, 0)
    greet(ep_peer(nz - 1, 1), tp)
    for d in range(1, nx):
        greet(ep, x_peer(d))
    for d in range(1, ny):
        greet(ep, y_peer(d))

    pair = col(tp // 2)
    loads = [
        pltpu.make_async_copy(tokens.at[:, pair], tok_in, in_sem.at[0]),
        pltpu.make_async_copy(cotangent.at[:, pair], cot_in, in_sem.at[1]),
        pltpu.make_async_copy(gate_w, gate_in, in_sem.at[2]),
        pltpu.make_async_copy(up_w, up_in, in_sem.at[3]),
        pltpu.make_async_copy(down_w, down_in, in_sem.at[4]),
    ]
    for load in loads:
        load.start()

    ids = lax.broadcasted_iota(jnp.int32, (nep, tok_dev), 0)
    first = (routes[0:1, :] == ids).astype(F32)
    second = (routes[1:2, :] == ids).astype(F32)
    named = first + second
    below = (
        lax.broadcasted_iota(jnp.int32, (tok_dev, tok_dev), 0)
        < lax.broadcasted_iota(jnp.int32, (tok_dev, tok_dev), 1)
    ).astype(F32).astype(BF16)
    place = dot(named.astype(BF16), below, 1, 0)
    at_slot = lax.broadcasted_iota(jnp.int32, (nep, cap, tok_dev), 1).astype(F32)

    def spread(value):
        return jnp.broadcast_to(value[:, None, :], (nep, cap, tok_dev))

    hit = (spread(place) == at_slot).astype(F32)
    hot0 = (hit * spread(first)).reshape(count, tok_dev)
    hot1 = (hit * spread(second)).reshape(count, tok_dev)
    onehot0[...] = hot0.astype(BF16)
    onehot1[...] = hot1.astype(BF16)
    row_w = jnp.sum(hot0 * weights[0:1, :] + hot1 * weights[1:2, :], axis=1, keepdims=True)

    loads[0].wait()
    loads[1].wait()
    lane = lax.broadcasted_iota(jnp.int32, (tok_dev, LANES), 1)
    odd = tp % 2
    tok = tok_in[...].astype(F32)
    cot = cot_in[...].astype(F32)
    tok = jnp.where(odd == 1, pltpu.roll(tok, FEAT, 1), tok)
    cot = jnp.where(odd == 1, cot, pltpu.roll(cot, FEAT, 1))
    both = jnp.where(lane < FEAT, tok, cot).astype(BF16)
    sent = dot((hot0 + hot1).astype(BF16), both, 1, 0)
    row_lane = lax.broadcasted_iota(jnp.int32, (count, LANES), 1)
    send[...] = (sent * jnp.where(row_lane < FEAT, 1.0, row_w)).astype(BF16)

    pl.semaphore_wait(barrier, (nep - 1) + (nx - 1) + (ny - 1))

    group = nep // CHUNKS
    my_group = ep // group

    def dispatch(i, c):
        to = ep_peer(i, c)
        remote(
            send.at[slot(to), :], rows.at[slot(ep), col(y)], z_send, z_recv.at[my_group], to, tp
        ).start()

    def dispatch_both(i, carry):
        dispatch(i, 0)
        dispatch(i, 1)
        return carry

    lax.fori_loop(0, nz - 1, dispatch_both, 0)
    dispatch(nz - 1, 1)
    rows[slot(ep), col(y)] = send[slot(ep), :]

    for load in loads[2:]:
        load.wait()
    w_lane = lax.broadcasted_iota(jnp.int32, (HID, LANES), 1)
    zero = jnp.zeros((HID, LANES), F32)
    for t in range(nx * ny):
        tile = slice(t // 2 * LANES, (t // 2 + 1) * LANES)
        to_x, to_tile = t % nx, slice(t // nx * LANES, (t // nx + 1) * LANES)
        for k, ref in enumerate((gate_in, up_in, down_in)):
            value = ref[:, tile].astype(F32)
            if (t % 2 == 0) == (k == 2):
                value = pltpu.roll(value, FEAT, 1)
            keep = (w_lane >= FEAT) if k == 2 else (w_lane < FEAT)
            w_send[to_x, k * HID : (k + 1) * HID, to_tile] = jnp.where(keep, value, zero).astype(BF16)
    w_rows = 3 * HID

    def w_place(i):
        return pl.ds(pl.multiple_of(i * LANES, LANES), w_rows)

    w_copies = []
    for d in range(1, nx):
        to = (x + d) % nx
        copy = remote(
            w_send.at[to], w_all.at[w_place(x), :], w_ssem.at[d], w_rsem.at[d], ep, x_peer(d)
        )
        copy.start()
        w_copies.append(copy)
    w_all[w_place(x), :] = w_send[x]
    for i in range(nx):
        w_all[i * LANES + w_rows : (i + 1) * LANES, :] = jnp.zeros((LANES - w_rows, ny * LANES), BF16)

    steps = ny // 2
    per = count // CHUNKS
    order = [0, 1, 3, 2]

    def chunk_of(i):
        return (my_group + order[i]) % CHUNKS

    def ring(way, step, i, owner):
        place_ = rows.at[pl.ds(pl.multiple_of(chunk_of(i) * per, per), per), col(owner)]
        to = y_peer(1) if way == 0 else y_peer(ny - 1)
        return remote(
            place_, place_, ag_ssem.at[way, step - 1, i], ag_rsem.at[way, step - 1, i], ep, to
        )

    def owner_of(way, back_):
        return (y + ny - back_) % ny if way == 0 else (y + back_) % ny

    def travels(way, step, i):
        return step < steps or (i < CHUNKS // 2) == (way == 0)

    ring_copies = []
    for wave in range(1, steps + CHUNKS):
        for step in range(steps, 0, -1):
            i = wave - step
            if not 0 <= i < CHUNKS:
                continue
            if step == 1:
                chunk = chunk_of(i)
                place_ = rows.at[pl.ds(pl.multiple_of(chunk * per, per), per), col(y)]
                short = rows.at[pl.ds(0, per - cap), col(y)]
                if order[i] == 0:
                    arrived(short, z_recv.at[chunk])
                else:
                    arrived(place_, z_recv.at[chunk])
            for way in (0, 1):
                if step > 1:
                    ring(way, step - 1, i, owner_of(way, step - 1)).wait_recv()
                if travels(way, step, i):
                    copy = ring(way, step, i, owner_of(way, step - 1))
                    copy.start()
                    ring_copies.append(copy)
    for way in (0, 1):
        for i in range(CHUNKS):
            if travels(way, steps, i):
                ring(way, steps, i, owner_of(way, steps)).wait_recv()

    for d in range(1, nx):
        arrived(w_all.at[w_place((x + nx - d) % nx), :], w_rsem.at[d])
    part = dot(rows[...], w_all[...], 1, 1)
    part_send[...] = part.astype(BF16)
    part_copies = []
    for d in range(1, nx):
        copy = remote(
            part_send.at[:, col((x + d) % nx)], part_got.at[d], px_ssem.at[d], px_rsem.at[d],
            ep, x_peer(d),
        )
        copy.start()
        part_copies.append(copy)
    for i in range(nx):
        top = slice(i * LANES, i * LANES + 2 * HID)
        rest = slice(i * LANES + 2 * HID, (i + 1) * LANES)
        w_left[top, :] = w_all[top, :]
        w_left[rest, :] = jnp.zeros((LANES - 2 * HID, ny * LANES), BF16)
        w_right[rest, :] = jnp.zeros((LANES - 2 * HID, ny * LANES), BF16)
        for j in range(ny):
            tile = slice(j * LANES, (j + 1) * LANES)
            w_right[top, tile] = pltpu.roll(w_all[top, tile].astype(F32), FEAT, 1).astype(BF16)
    pre = part_send[:, col(x)].astype(F32)
    for d in range(1, nx):
        arrived(part_got.at[d], px_rsem.at[d])
        pre = pre + part_got[d].astype(F32)
    up = pltpu.roll(pre, LANES - HID, 1)
    d_hidden = pltpu.roll(pre, LANES - 2 * HID, 1)
    sig = jax.nn.sigmoid(pre)
    act = pre * sig * up
    d_gate = d_hidden * up * sig * (1.0 + pre * (1.0 - sig))
    d_up = d_hidden * pre * sig
    rw = jnp.sum(jnp.where(row_lane < HID, act * d_hidden, 0.0), axis=1, keepdims=True)
    packed = jnp.where(
        row_lane < HID,
        d_gate,
        jnp.where(
            row_lane < 2 * HID,
            pltpu.roll(d_up, HID, 1),
            jnp.where(
                row_lane < 3 * HID,
                pltpu.roll(act, 2 * HID, 1),
                jnp.where(row_lane == 3 * HID, rw, 0.0),
            ),
        ),
    )
    hidden[:, col(x)] = packed.astype(BF16)
    hidden_copies = []
    for d in range(1, nx):
        copy = remote(
            hidden.at[:, col(x)], hidden.at[:, col(x)], hx_ssem.at[d], hx_rsem.at[d], ep, x_peer(d)
        )
        copy.start()
        hidden_copies.append(copy)
    for d in range(1, nx):
        arrived(hidden.at[:, col((x + nx - d) % nx)], hx_rsem.at[d])

    pieces = dot(hidden[0:half, :], w_left[...], 1, 0) + dot(hidden[half:count, :], w_right[...], 1, 0)
    piece[...] = pieces.astype(BF16)
    pick = (lax.broadcasted_iota(jnp.int32, (16, nx * LANES), 1) % LANES == 3 * HID).astype(F32).astype(BF16)
    rw_row[...] = dot(pick, hidden[...], 1, 1)[0:1, :]
    y_order = []
    for k in range(ny - 1):
        y_order.append(ny // 2 + (k + 1) // 2 * (1 if k % 2 == 0 else -1))
    piece_copies = []
    for d in y_order:
        copy = remote(
            piece.at[:, col((y + d) % ny)], piece_got.at[d], ry_ssem.at[d], ry_rsem.at[d],
            ep, y_peer(d),
        )
        copy.start()
        piece_copies.append(copy)
        copy = remote(rw_row, rw_got.at[d], rw_ssem.at[d], rw_rsem.at[d], ep, y_peer(d))
        copy.start()
        piece_copies.append(copy)

    grads = dot(hidden[...], rows[...], 0, 0)
    g_lane = lax.broadcasted_iota(jnp.int32, (HID, ny * LANES), 1) % LANES
    for i in range(nx):
        at = i * LANES
        gate_down = jnp.where(g_lane < FEAT, grads[at : at + HID, :], grads[at + 2 * HID : at + 3 * HID, :])
        grad_send[i, 0:HID, :] = gate_down.astype(BF16)
        grad_send[i, HID : 2 * HID, :] = grads[at + HID : at + 2 * HID, :].astype(BF16)
    grad_copies = []
    for d in range(1, nx):
        copy = remote(
            grad_send.at[(x + d) % nx], grad_got.at[x], g_ssem.at[d], g_rsem.at[d], ep, x_peer(d)
        )
        copy.start()
        grad_copies.append(copy)
    grad_got[x] = grad_send[x]

    total = piece[:, col(y)].astype(F32)
    total_rw = rw_row[...]
    for d in y_order[::-1]:
        arrived(piece_got.at[d], ry_rsem.at[d])
        arrived(rw_got.at[d], rw_rsem.at[d])
        total = total + piece_got[d].astype(F32)
        total_rw = total_rw + rw_got[d]
    spread_rw = jnp.broadcast_to(total_rw, (LANES, count)).T
    total = jnp.concatenate([total, pltpu.roll(total, FEAT, 1)], axis=0)
    back[...] = jnp.where(row_lane < FEAT, total, spread_rw).astype(BF16)

    def send_back(i, c):
        to = ep_peer(i, c)
        remote(back.at[slot(to), :], back_got.at[slot(ep), :], b_ssem, b_rsem, to, tp).start()

    def back_both(i, carry):
        send_back(i, 0)
        send_back(i, 1)
        return carry

    lax.fori_loop(0, nz - 1, back_both, 0)
    send_back(nz - 1, 1)
    back_got[slot(ep), :] = back[slot(ep), :]

    for d in range(1, nx):
        arrived(grad_got.at[(x + nx - d) % nx], g_rsem.at[d])
    for t in range(0, nx * ny, 2):
        tile = slice(t // 2 * LANES, (t // 2 + 1) * LANES)
        src = slice(t // nx * LANES, (t // nx + 1) * LANES)
        a, b = t % nx, t % nx + 1
        top_a = grad_got[a, 0:HID, src].astype(F32)
        top_b = grad_got[b, 0:HID, src].astype(F32)
        up_a = grad_got[a, HID : 2 * HID, src].astype(F32)
        up_b = grad_got[b, HID : 2 * HID, src].astype(F32)
        out_gate[:, tile] = jnp.where(w_lane < FEAT, top_a, pltpu.roll(top_b, FEAT, 1))
        out_up[:, tile] = jnp.where(w_lane < FEAT, up_a, pltpu.roll(up_b, FEAT, 1))
        out_down[:, tile] = jnp.where(w_lane < FEAT, pltpu.roll(top_a, FEAT, 1), top_b)

    others = pl.ds(0, (nep - 1) * cap)
    arrived(back_got.at[others, :], b_rsem)
    got = back_got[...]
    by_first = dot(got, onehot0[...], 0, 0)
    by_second = dot(got, onehot1[...], 0, 0)
    out_tok[...] = (by_first[0:FEAT, :] + by_second[0:FEAT, :]).astype(BF16)
    out_rw[0:1, :] = by_first[FEAT : FEAT + 1, :] / weights[0:1, :]
    out_rw[1:2, :] = by_second[FEAT : FEAT + 1, :] / weights[1:2, :]

    arrived(send.at[others, :], z_send)
    arrived(back.at[others, :], b_ssem)
    for copy in w_copies + ring_copies + part_copies + hidden_copies + piece_copies + grad_copies:
        copy.wait_send()


def on_device(nz, ny, nx, tokens, cotangent, routes, route_weight, w_gate, w_up, w_down):
    tok_dev, model = tokens.shape
    hid = w_down.shape[1]
    nep = 2 * nz
    cap = 2 * tok_dev * routes.shape[1] // nep
    count = nep * cap
    half = count // 2
    wide_x, wide_y = nx * LANES, ny * LANES
    steps = ny // 2
    any_ = pl.BlockSpec(memory_space=pl.ANY)
    vmem = pl.BlockSpec(memory_space=pltpu.VMEM)
    dma = pltpu.SemaphoreType.DMA
    outs = pl.pallas_call(
        functools.partial(kernel, nz, ny, nx, cap),
        out_shape=(
            jax.ShapeDtypeStruct((FEAT, tok_dev), BF16),
            jax.ShapeDtypeStruct((2, tok_dev), F32),
            jax.ShapeDtypeStruct((hid, model), F32),
            jax.ShapeDtypeStruct((hid, model), F32),
            jax.ShapeDtypeStruct((hid, model), F32),
        ),
        in_specs=[any_, any_, vmem, vmem, any_, any_, any_],
        out_specs=[vmem] * 5,
        scratch_shapes=[
            pltpu.VMEM((tok_dev, LANES), BF16),
            pltpu.VMEM((tok_dev, LANES), BF16),
            pltpu.VMEM((hid, model), BF16),
            pltpu.VMEM((hid, model), BF16),
            pltpu.VMEM((hid, model), BF16),
            pltpu.VMEM((count, tok_dev), BF16),
            pltpu.VMEM((count, tok_dev), BF16),
            pltpu.VMEM((count, LANES), BF16),
            pltpu.VMEM((count, wide_y), BF16),
            pltpu.VMEM((nx, 3 * HID, wide_y), BF16),
            pltpu.VMEM((wide_x, wide_y), BF16),
            pltpu.VMEM((wide_x, wide_y), BF16),
            pltpu.VMEM((wide_x, wide_y), BF16),
            pltpu.VMEM((count, wide_x), BF16),
            pltpu.VMEM((nx, count, LANES), BF16),
            pltpu.VMEM((count, wide_x), BF16),
            pltpu.VMEM((half, wide_y), BF16),
            pltpu.VMEM((ny, half, LANES), BF16),
            pltpu.VMEM((1, count), F32),
            pltpu.VMEM((ny, 1, count), F32),
            pltpu.VMEM((count, LANES), BF16),
            pltpu.VMEM((count, LANES), BF16),
            pltpu.VMEM((nx, 2 * HID, wide_y), BF16),
            pltpu.VMEM((nx, 2 * HID, wide_y), BF16),
            dma((5,)),
            dma,
            dma((CHUNKS,)),
            dma((nx,)),
            dma((nx,)),
            dma((2, steps, CHUNKS)),
            dma((2, steps, CHUNKS)),
            dma((nx,)),
            dma((nx,)),
            dma((nx,)),
            dma((nx,)),
            dma((ny,)),
            dma((ny,)),
            dma((ny,)),
            dma((ny,)),
            dma,
            dma,
            dma((nx,)),
            dma((nx,)),
        ],
        compiler_params=pltpu.CompilerParams(
            collective_id=0, has_side_effects=True, vmem_limit_bytes=48 * 1024 * 1024
        ),
        name="experts_backward",
    )(
        tokens,
        cotangent,
        routes.T,
        route_weight.T,
        w_gate[0].T,
        w_up[0].T,
        w_down[0],
    )
    g_tok, g_rw, g_gate, g_up, g_down = outs
    return g_tok.T, g_rw.T, g_gate.T[None], g_up.T[None], g_down[None]


def solution(mesh):
    nz = mesh.shape["ep"] // 2
    nx = 4 if mesh.shape["tp"] >= 16 else 2
    ny = mesh.shape["tp"] // nx
    return jax.shard_map(
        functools.partial(on_device, nz, ny, nx),
        mesh=mesh,
        in_specs=(
            P("ep", None),
            P("ep", None),
            P("ep", None),
            P("ep", None),
            P("ep", None, "tp"),
            P("ep", None, "tp"),
            P("ep", "tp", None),
        ),
        out_specs=(
            P("ep", "tp"),
            P("ep", None),
            P("ep", None, "tp"),
            P("ep", None, "tp"),
            P("ep", "tp", None),
        ),
        check_vma=False,
    )
```

time: 290 us -> 103 us (0.36)
  waiting for transfers between devices: 152 us -> 0 us
  Pallas kernels: 0 us -> 93.3 us
  starting transfers between devices: 62.6 us -> 0 us
  local copies, waits for them, and re-layouts: 29.4 us -> 8.75 us
  blocking collectives: 16.2 us -> 0 us
  between operations: 14.3 us -> 0.67 us
  matrix products: 10.2 us -> 0 us
  other arithmetic: 3.77 us -> 0 us
    pallas_call x0 -> x1, Pallas kernels: none -> 93.3 us  [on_device(): pl.pallas_call(functools.partial(kernel, nz, ny, nx, cap), out_shape=(jax...]
    all_to_all x6 -> x0, waiting for transfers between devices: 83.9 us -> none  [the longest x1 41.2 us: summed_on_arrival(): lax.all_to_all(in_blocks(value, dim, length), axis, 0, 0, tiled=True)]
    all_gather x1 -> x0, waiting for transfers between devices: 68.4 us -> none  [rows_first(): lax.all_gather(both, axis, axis=0, tiled=True)]
    all_to_all x6 -> x0, starting transfers between devices: 62.6 us -> none  [the longest x1 20.4 us: on_device(): lax.all_to_all(send_dy.reshape(experts, capacity, share), 'ep', split_axi...]
    all_to_all x1 -> x0, blocking collectives: 16.2 us -> none  [on_device(): lax.all_to_all(send_w.reshape(experts, capacity, 1).astype(jnp.bfloat16),...]
    dot_general x8 -> x0, matrix products: 10.2 us -> none  [the longest x1 2.91 us: on_device(): jnp.einsum('rf,rd->fd', act, weighted_cot, preferred_element_type=f32)[None]]
    convert_element_type x4 -> x0, local copies, waits for them, and re-layouts: 4.8 us -> none  [the longest x1 3.93 us: on_device(): rounded_part = token_part.astype(jnp.bfloat16).astype(f32)]
    slice x2 -> x0, local copies, waits for them, and re-layouts: 4 us -> none  [the longest x1 3.82 us: rows_first(): share = whole[:, at:at + t[0].size].reshape(-1, *t.shape[1:])]
  transfers between devices with their start and end apart: 7 -> 0, of which waited for: 7 -> 0; matrix products, arithmetic and copies ran while one was open for 8% -> 0% of each run, Pallas kernels for 0% -> 0%
where the time goes in v1:
time: 103 us
  Pallas kernels  93.3 us (91%)
  local copies, waits for them, and re-layouts  8.75 us (8%)
    pallas_call x1, Pallas kernels, on_device(): pl.pallas_call(functools.partial(kernel, nz, ny, nx, cap), out_shape=(jax...  93.3 us
    unnamed x19, local copies, waits for them, and re-layouts  8.75 us

profile of v1, /device:TPU:1, one launch (start us, length us, event | category | flops | bytes accessed | tf_op | source)
XLA Modules:
  0.0 102.7 jit_solution(7494087267933070308)
XLA Ops:
  0.6 0.0 copy-start.6
  0.6 0.0 copy-start.5
  0.7 0.7 copy-done.6
  1.3 0.0 copy-done.5
  1.3 0.0 copy-start
  1.3 1.0 %copy-done = bf16[128,2048]{1,0:T(8,128)(2,1)S(1)} copy-done((bf16[128,2048]{1,0:T(8,128)(2,1)S(1)}, bf16[128,2048]{1,0:T(8,128)(2,1)}, u32[]{:S(2)}) %copy-start) | copy-done | bytes 524312
  2.4 0.0 copy-start.1
  2.4 1.0 %copy-done.1 = bf16[128,2048]{1,0:T(8,128)(2,1)S(1)} copy-done((bf16[128,2048]{1,0:T(8,128)(2,1)S(1)}, bf16[128,2048]{1,0:T(8,128)(2,1)}, u32[]{:S(2)}) %copy-start.1) | copy-done | bytes 524312
  3.4 0.0 copy-start.2
  3.4 0.9 copy-done.2
  4.3 0.0 copy-start.3
  4.3 0.9 copy-done.3
  5.2 0.0 copy-start.4
  5.2 0.9 copy-done.4
  6.1 93.3 %experts_backward.1 = (bf16[64,128]{1,0:T(8,128)(2,1)S(1)}, f32[2,128]{1,0:T(2,128)S(1)}, f32[32,2048]{1,0:T(8,128)S(1)}, f32[32,2048]{1,0:T(8,128)S(1)}, f32[32,2048]{1,0:T(8,128)S(1)}) custom-call(bf16[128,2048]{1,0:T(8,128)(2,1)S(1)} %copy-done, bf16[128,2048]{1,0:T(8,128)(2,1)S(1)} %copy-done.1, s32[2,128]{1,0:T(2,128)S(1)} %bitcast.26, ...), custom_call_target="tpu_custom_call" | custom-call | tf_op jit(solution)/shard_map/experts_backward/pallas_call | solution.py:384
  99.4 0.6 copy.17
  100.0 0.6 copy.18
  100.6 0.7 copy.19
  101.3 0.7 copy.20
  102.0 0.7 copy.21
Async XLA Ops:
  0.6 0.7 copy-start.6
  0.6 0.7 copy-start.5
  1.3 1.0 %copy-start = (bf16[128,2048]{1,0:T(8,128)(2,1)S(1)}, bf16[128,2048]{1,0:T(8,128)(2,1)}, u32[]{:S(2)}) copy-start(bf16[128,2048]{1,0:T(8,128)(2,1)} %tokens.1) | copy-start | bytes 1572868
  2.4 1.0 %copy-start.1 = (bf16[128,2048]{1,0:T(8,128)(2,1)S(1)}, bf16[128,2048]{1,0:T(8,128)(2,1)}, u32[]{:S(2)}) copy-start(bf16[128,2048]{1,0:T(8,128)(2,1)} %cotangent.1) | copy-start | bytes 1572868
  3.4 0.9 copy-start.2
  4.3 0.9 copy-start.3
  5.2 0.9 copy-start.4

commit v2 on v1

v2 whole, which is shorter than its diff:
```python
import functools

import jax
import jax.numpy as jnp
from jax import lax
from jax.experimental import pallas as pl
from jax.experimental.pallas import tpu as pltpu
from jax.sharding import PartitionSpec as P

MESH = pl.DeviceIdType.MESH
F32 = jnp.float32
BF16 = jnp.bfloat16
LANES = 128
FEAT = 64
HID = 32
CHUNKS = 4


def dot(a, b, ca, cb):
    return lax.dot_general(a, b, (((ca,), (cb,)), ((), ())), preferred_element_type=F32)


def kernel(
    nz, ny, nx, cap,
    tokens, cotangent, routes_in, weights_in, gate_w, up_w, down_w,
    *refs,
):
    (
        out_hbm0, out_hbm1, out_hbm2, out_hbm3, out_hbm4,
        tok_in, cot_in, gate_in, up_in, down_in, routes, weights,
        onehot0, onehot1, send, rows, w_send, w_all, w_left,
        part_send, part_got, hidden, piece, piece_got, rw_row, rw_got,
        back, back_got, grad_send, grad_got,
        in_sem, z_send, z_recv, w_ssem, w_rsem, ag_ssem, ag_rsem,
        px_ssem, px_rsem, hx_ssem, hx_rsem, ry_ssem, ry_rsem, rw_ssem, rw_rsem,
        b_ssem, b_rsem, g_ssem, g_rsem,
        out_tok, out_rw, out_gate, out_up, out_down, out_sem,
    ) = refs
    nep = 2 * nz
    count = nep * cap
    tok_dev = tokens.shape[0]
    ep = lax.axis_index("ep")
    tp = lax.axis_index("tp")
    z, core = ep // 2, ep % 2
    y, x = tp // nx, tp % nx

    def remote(src, dst, ssem, rsem, to_ep, to_tp):
        return pltpu.make_async_remote_copy(
            src_ref=src, dst_ref=dst, send_sem=ssem, recv_sem=rsem,
            device_id=(to_ep, to_tp), device_id_type=MESH,
        )

    def arrived(ref, sem):
        pltpu.make_async_copy(ref, ref, sem).wait()

    def ep_peer(i, c):
        k = (i + 1) // 2
        dz = nz // 2 + k - 2 * k * (i % 2)
        return ((z + dz) % nz) * 2 + (core + c) % 2

    def x_peer(d):
        return y * nx + (x + d) % nx

    def y_peer(d):
        return ((y + d) % ny) * nx + x

    def col(i):
        return pl.ds(pl.multiple_of(i * LANES, LANES), LANES)

    def slot(e):
        return pl.ds(pl.multiple_of(e * cap, cap), cap)

    barrier = pltpu.get_barrier_semaphore()

    def greet(to_ep, to_tp):
        pl.semaphore_signal(barrier, inc=1, device_id=(to_ep, to_tp), device_id_type=MESH)

    def greet_ep(i, carry):
        greet(ep_peer(i, 0), tp)
        greet(ep_peer(i, 1), tp)
        return carry

    lax.fori_loop(0, nz - 1, greet_ep, 0)
    greet(ep_peer(nz - 1, 1), tp)
    for d in range(1, nx):
        greet(ep, x_peer(d))
    for d in range(1, ny):
        greet(ep, y_peer(d))

    pair = col(tp // 2)
    loads = [
        pltpu.make_async_copy(tokens.at[:, pair], tok_in, in_sem.at[0]),
        pltpu.make_async_copy(cotangent.at[:, pair], cot_in, in_sem.at[1]),
        pltpu.make_async_copy(gate_w, gate_in, in_sem.at[2]),
        pltpu.make_async_copy(up_w, up_in, in_sem.at[3]),
        pltpu.make_async_copy(down_w, down_in, in_sem.at[4]),
        pltpu.make_async_copy(routes_in, routes, in_sem.at[5]),
        pltpu.make_async_copy(weights_in, weights, in_sem.at[6]),
    ]
    for load in loads[5:] + loads[:5]:
        load.start()
    loads[5].wait()
    loads[6].wait()

    ids = lax.broadcasted_iota(jnp.int32, (nep, tok_dev), 0)
    first = (routes[0:1, :] == ids).astype(F32)
    second = (routes[1:2, :] == ids).astype(F32)
    named = first + second
    below = (
        lax.broadcasted_iota(jnp.int32, (tok_dev, tok_dev), 0)
        < lax.broadcasted_iota(jnp.int32, (tok_dev, tok_dev), 1)
    ).astype(F32).astype(BF16)
    place = dot(named.astype(BF16), below, 1, 0)
    at_slot = lax.broadcasted_iota(jnp.int32, (nep, cap, tok_dev), 1).astype(F32)

    def spread(value):
        return jnp.broadcast_to(value[:, None, :], (nep, cap, tok_dev))

    hit = (spread(place) == at_slot).astype(F32)
    hot0 = (hit * spread(first)).reshape(count, tok_dev)
    hot1 = (hit * spread(second)).reshape(count, tok_dev)
    onehot0[...] = hot0.astype(BF16)
    onehot1[...] = hot1.astype(BF16)
    row_w = jnp.sum(hot0 * weights[0:1, :] + hot1 * weights[1:2, :], axis=1, keepdims=True)

    loads[0].wait()
    loads[1].wait()
    lane = lax.broadcasted_iota(jnp.int32, (tok_dev, LANES), 1)
    odd = tp % 2
    tok = tok_in[...].astype(F32)
    cot = cot_in[...].astype(F32)
    tok = jnp.where(odd == 1, pltpu.roll(tok, FEAT, 1), tok)
    cot = jnp.where(odd == 1, cot, pltpu.roll(cot, FEAT, 1))
    both = jnp.where(lane < FEAT, tok, cot).astype(BF16)
    sent = dot((hot0 + hot1).astype(BF16), both, 1, 0)
    row_lane = lax.broadcasted_iota(jnp.int32, (count, LANES), 1)
    send[...] = (sent * jnp.where(row_lane < FEAT, 1.0, row_w)).astype(BF16)

    pl.semaphore_wait(barrier, (nep - 1) + (nx - 1) + (ny - 1))

    group = nep // CHUNKS
    my_group = ep // group

    def dispatch(i, c):
        to = ep_peer(i, c)
        remote(
            send.at[slot(to), :], rows.at[slot(ep), col(y)], z_send, z_recv.at[my_group], to, tp
        ).start()

    def dispatch_both(i, carry):
        dispatch(i, 0)
        dispatch(i, 1)
        return carry

    lax.fori_loop(0, nz - 1, dispatch_both, 0)
    dispatch(nz - 1, 1)
    rows[slot(ep), col(y)] = send[slot(ep), :]

    for load in loads[2:5]:
        load.wait()
    w_lane = lax.broadcasted_iota(jnp.int32, (HID, LANES), 1)
    zero = jnp.zeros((HID, LANES), F32)
    for t in range(nx * ny):
        tile = slice(t // 2 * LANES, (t // 2 + 1) * LANES)
        to_x, to_tile = t % nx, slice(t // nx * LANES, (t // nx + 1) * LANES)
        for k, ref in enumerate((gate_in, up_in, down_in)):
            value = ref[:, tile].astype(F32)
            if (t % 2 == 0) == (k == 2):
                value = pltpu.roll(value, FEAT, 1)
            keep = (w_lane >= FEAT) if k == 2 else (w_lane < FEAT)
            w_send[to_x, k * HID : (k + 1) * HID, to_tile] = jnp.where(keep, value, zero).astype(BF16)
    w_rows = 3 * HID

    def w_place(i):
        return pl.ds(pl.multiple_of(i * LANES, LANES), w_rows)

    w_copies = []
    for d in range(1, nx):
        to = (x + d) % nx
        copy = remote(
            w_send.at[to], w_all.at[w_place(x), :], w_ssem.at[d], w_rsem.at[d], ep, x_peer(d)
        )
        copy.start()
        w_copies.append(copy)
    w_all[w_place(x), :] = w_send[x]
    for i in range(nx):
        w_all[i * LANES + w_rows : (i + 1) * LANES, :] = jnp.zeros((LANES - w_rows, ny * LANES), BF16)

    steps = ny // 2
    per = count // CHUNKS
    pack = per // 2
    order = [0, 1, 3, 2]
    lane_c = lax.broadcasted_iota(jnp.int32, (per, LANES), 1)
    lane_p = lax.broadcasted_iota(jnp.int32, (pack, LANES), 1)
    pick = (lax.broadcasted_iota(jnp.int32, (16, nx * LANES), 1) % LANES == 3 * HID).astype(F32).astype(BF16)
    y_order = [ny // 2 + (k + 1) // 2 * (1 if k % 2 == 0 else -1) for k in range(ny - 1)]
    copies = []

    def launch(copy):
        copy.start()
        copies.append(copy)

    def chunk_of(i):
        return (my_group + order[i]) % CHUNKS

    def chunk_rows(i):
        return pl.ds(pl.multiple_of(chunk_of(i) * per, per), per)

    def ring(way, step, i, owner):
        block = rows.at[chunk_rows(i), col(owner)]
        to = y_peer(1) if way == 0 else y_peer(ny - 1)
        return remote(
            block, block, ag_ssem.at[way, step - 1, i], ag_rsem.at[way, step - 1, i], ep, to
        )

    def owner_of(way, hops):
        return (y + ny - hops) % ny if way == 0 else (y + hops) % ny

    def travels(way, step, i):
        return step < steps or (i < CHUNKS // 2) == (way == 0)

    def gather(i, step):
        if step == 1:
            if order[i] == 0:
                arrived(rows.at[pl.ds(0, per - cap), col(y)], z_recv.at[chunk_of(i)])
            else:
                arrived(rows.at[chunk_rows(i), col(y)], z_recv.at[chunk_of(i)])
        for way in (0, 1):
            if step > 1 and travels(way, step - 1, i):
                ring(way, step - 1, i, owner_of(way, step - 1)).wait_recv()
            if step <= steps and travels(way, step, i):
                launch(ring(way, step, i, owner_of(way, step - 1)))

    def partial(i):
        gather(i, steps + 1)
        if i == 0:
            for d in range(1, nx):
                arrived(w_all.at[w_place((x + nx - d) % nx), :], w_rsem.at[d])
        part_send[i] = dot(rows[chunk_rows(i), :], w_all[...], 1, 1).astype(BF16)
        for d in x_order:
            launch(
                remote(
                    part_send.at[i, :, col((x + d) % nx)], part_got.at[d, i],
                    px_ssem.at[d, i], px_rsem.at[d, i], ep, x_peer(d),
                )
            )
        if i == 0:
            for k in range(nx):
                top = slice(k * LANES, k * LANES + 2 * HID)
                rest = slice(k * LANES + 2 * HID, (k + 1) * LANES)
                w_left[top, :] = w_all[top, :]
                w_left[rest, :] = jnp.zeros((LANES - 2 * HID, ny * LANES), BF16)

    def activate(i):
        pre = part_send[i, :, col(x)].astype(F32)
        for d in range(1, nx):
            arrived(part_got.at[d, i], px_rsem.at[d, i])
            pre = pre + part_got[d, i].astype(F32)
        up = pltpu.roll(pre, LANES - HID, 1)
        d_hidden = pltpu.roll(pre, LANES - 2 * HID, 1)
        sig = jax.nn.sigmoid(pre)
        act = pre * sig * up
        d_gate = d_hidden * up * sig * (1.0 + pre * (1.0 - sig))
        d_up = d_hidden * pre * sig
        rw = jnp.sum(jnp.where(lane_c < HID, act * d_hidden, 0.0), axis=1, keepdims=True)
        tail = jnp.where(lane_c == 3 * HID, rw, 0.0)
        packed = jnp.where(lane_c < 3 * HID, pltpu.roll(act, 2 * HID, 1), tail)
        packed = jnp.where(lane_c < 2 * HID, pltpu.roll(d_up, HID, 1), packed)
        packed = jnp.where(lane_c < HID, d_gate, packed)
        mine = hidden.at[chunk_rows(i), col(x)]
        hidden[chunk_rows(i), col(x)] = packed.astype(BF16)
        for d in x_order:
            launch(remote(mine, mine, hx_ssem.at[d, i], hx_rsem.at[d, i], ep, x_peer(d)))

    def token_part(i):
        for d in range(1, nx):
            arrived(hidden.at[chunk_rows(i), col((x + nx - d) % nx)], hx_rsem.at[d, i])
        value = hidden[chunk_rows(i), :]
        whole = dot(value, w_left[...], 1, 0)
        for j in range(ny):
            tile = slice(j * LANES, (j + 1) * LANES)
            right = pltpu.roll(whole[pack:per, tile], FEAT, 1)
            piece[i, :, tile] = jnp.where(lane_p < FEAT, whole[0:pack, tile], right).astype(BF16)
        rw_row[i] = dot(pick, value, 1, 1)[0:1, :]
        for d in y_order:
            launch(
                remote(
                    piece.at[i, :, col((y + d) % ny)], piece_got.at[d, i],
                    ry_ssem.at[d, i], ry_rsem.at[d, i], ep, y_peer(d),
                )
            )
            launch(
                remote(rw_row.at[i], rw_got.at[d, i], rw_ssem.at[d, i], rw_rsem.at[d, i], ep, y_peer(d))
            )

    def send_back(to):
        remote(back.at[slot(to), :], back_got.at[slot(ep), :], b_ssem, b_rsem, to, tp).start()

    def summed(i):
        total = piece[i, :, col(y)].astype(F32)
        total_rw = rw_row[i]
        for d in y_order[::-1]:
            arrived(piece_got.at[d, i], ry_rsem.at[d, i])
            arrived(rw_got.at[d, i], rw_rsem.at[d, i])
            total = total + piece_got[d, i].astype(F32)
            total_rw = total_rw + rw_got[d, i]
        spread_rw = jnp.broadcast_to(total_rw, (per, per)).T
        both_ = jnp.concatenate([total, pltpu.roll(total, FEAT, 1)], axis=0)
        if per < LANES:
            spread_rw = jnp.broadcast_to(spread_rw[:, 0:1], (per, LANES))
        back[chunk_rows(i), :] = jnp.where(lane_c < FEAT, both_, spread_rw).astype(BF16)
        base = chunk_of(i) * group
        if order[i] == 0:
            back_got[slot(ep), :] = back[slot(ep), :]
        for j in range(1 if order[i] == 0 else 0, group):
            send_back(base + (ep + j) % group)

    x_order = list(range(1, nx))
    stages = [functools.partial(gather, step=s) for s in range(1, steps + 1)]
    stages += [partial, activate, token_part, summed]
    for wave in range(len(stages) + CHUNKS - 1):
        if wave == len(stages) + CHUNKS - 2:
            grads = dot(hidden[...], rows[...], 0, 0)
            g_lane = lax.broadcasted_iota(jnp.int32, (HID, ny * LANES), 1) % LANES
            for k in range(nx):
                at = k * LANES
                gate_down = jnp.where(
                    g_lane < FEAT, grads[at : at + HID, :], grads[at + 2 * HID : at + 3 * HID, :]
                )
                grad_send[k, 0:HID, :] = gate_down.astype(BF16)
                grad_send[k, HID : 2 * HID, :] = grads[at + HID : at + 2 * HID, :].astype(BF16)
            for d in range(1, nx):
                launch(
                    remote(
                        grad_send.at[(x + d) % nx], grad_got.at[x], g_ssem.at[d], g_rsem.at[d],
                        ep, x_peer(d),
                    )
                )
            grad_got[x] = grad_send[x]
        for k, stage in enumerate(stages):
            if 0 <= wave - k < CHUNKS:
                stage(wave - k)

    for d in range(1, nx):
        arrived(grad_got.at[(x + nx - d) % nx], g_rsem.at[d])
    for t in range(0, nx * ny, 2):
        tile = slice(t // 2 * LANES, (t // 2 + 1) * LANES)
        src = slice(t // nx * LANES, (t // nx + 1) * LANES)
        a, b = t % nx, t % nx + 1
        top_a = grad_got[a, 0:HID, src].astype(F32)
        top_b = grad_got[b, 0:HID, src].astype(F32)
        up_a = grad_got[a, HID : 2 * HID, src].astype(F32)
        up_b = grad_got[b, HID : 2 * HID, src].astype(F32)
        out_gate[:, tile] = jnp.where(w_lane < FEAT, top_a, pltpu.roll(top_b, FEAT, 1))
        out_up[:, tile] = jnp.where(w_lane < FEAT, up_a, pltpu.roll(up_b, FEAT, 1))
        out_down[:, tile] = jnp.where(w_lane < FEAT, pltpu.roll(top_a, FEAT, 1), top_b)

    stores = [
        pltpu.make_async_copy(out_tok, out_hbm0, out_sem.at[0]),
        pltpu.make_async_copy(out_rw, out_hbm1, out_sem.at[1]),
        pltpu.make_async_copy(out_gate, out_hbm2, out_sem.at[2]),
        pltpu.make_async_copy(out_up, out_hbm3, out_sem.at[3]),
        pltpu.make_async_copy(out_down, out_hbm4, out_sem.at[4]),
    ]
    for copy in stores[2:]:
        copy.start()
    others = pl.ds(0, (nep - 1) * cap)
    arrived(back_got.at[others, :], b_rsem)
    got = back_got[...]
    by_first = dot(got, onehot0[...], 0, 0)
    by_second = dot(got, onehot1[...], 0, 0)
    out_tok[...] = (by_first[0:FEAT, :] + by_second[0:FEAT, :]).astype(BF16)
    out_rw[0:1, :] = by_first[FEAT : FEAT + 1, :] / weights[0:1, :]
    out_rw[1:2, :] = by_second[FEAT : FEAT + 1, :] / weights[1:2, :]

    for copy in stores[:2]:
        copy.start()
    arrived(send.at[others, :], z_send)
    arrived(back.at[others, :], b_ssem)
    for copy in w_copies + copies:
        copy.wait_send()
    for copy in stores:
        copy.wait()


def store(*refs):
    given, kept, held, sems = refs[0:5], refs[5:10], refs[10:15], refs[15]
    loads = [pltpu.make_async_copy(given[i], held[i], sems.at[0, i]) for i in range(5)]
    stores = [pltpu.make_async_copy(held[i], kept[i], sems.at[1, i]) for i in range(5)]
    for copy in loads:
        copy.start()
    for load, copy in zip(loads, stores):
        load.wait()
        copy.start()
    for copy in stores:
        copy.wait()


def on_device(nz, ny, nx, tokens, cotangent, routes, route_weight, w_gate, w_up, w_down):
    tok_dev, model = tokens.shape
    hid = w_down.shape[1]
    nep = 2 * nz
    cap = 2 * tok_dev * routes.shape[1] // nep
    count = nep * cap
    per = count // CHUNKS
    wide_x, wide_y = nx * LANES, ny * LANES
    steps = ny // 2
    hbm = pl.BlockSpec(memory_space=pltpu.HBM)
    dma = pltpu.SemaphoreType.DMA
    outs = pl.pallas_call(
        functools.partial(kernel, nz, ny, nx, cap),
        out_shape=(
            jax.ShapeDtypeStruct((FEAT, tok_dev), BF16),
            jax.ShapeDtypeStruct((2, tok_dev), F32),
            jax.ShapeDtypeStruct((hid, model), F32),
            jax.ShapeDtypeStruct((hid, model), F32),
            jax.ShapeDtypeStruct((hid, model), F32),
        ),
        in_specs=[hbm] * 7,
        out_specs=[hbm] * 5,
        scratch_shapes=[
            pltpu.VMEM((tok_dev, LANES), BF16),
            pltpu.VMEM((tok_dev, LANES), BF16),
            pltpu.VMEM((hid, model), BF16),
            pltpu.VMEM((hid, model), BF16),
            pltpu.VMEM((hid, model), BF16),
            pltpu.VMEM((2, tok_dev), jnp.int32),
            pltpu.VMEM((2, tok_dev), F32),
            pltpu.VMEM((count, tok_dev), BF16),
            pltpu.VMEM((count, tok_dev), BF16),
            pltpu.VMEM((count, LANES), BF16),
            pltpu.VMEM((count, wide_y), BF16),
            pltpu.VMEM((nx, 3 * HID, wide_y), BF16),
            pltpu.VMEM((wide_x, wide_y), BF16),
            pltpu.VMEM((wide_x, wide_y), BF16),
            pltpu.VMEM((CHUNKS, per, wide_x), BF16),
            pltpu.VMEM((nx, CHUNKS, per, LANES), BF16),
            pltpu.VMEM((count, wide_x), BF16),
            pltpu.VMEM((CHUNKS, per // 2, wide_y), BF16),
            pltpu.VMEM((ny, CHUNKS, per // 2, LANES), BF16),
            pltpu.VMEM((CHUNKS, 1, per), F32),
            pltpu.VMEM((ny, CHUNKS, 1, per), F32),
            pltpu.VMEM((count, LANES), BF16),
            pltpu.VMEM((count, LANES), BF16),
            pltpu.VMEM((nx, 2 * HID, wide_y), BF16),
            pltpu.VMEM((nx, 2 * HID, wide_y), BF16),
            dma((7,)),
            dma,
            dma((CHUNKS,)),
            dma((nx,)),
            dma((nx,)),
            dma((2, steps, CHUNKS)),
            dma((2, steps, CHUNKS)),
            dma((nx, CHUNKS)),
            dma((nx, CHUNKS)),
            dma((nx, CHUNKS)),
            dma((nx, CHUNKS)),
            dma((ny, CHUNKS)),
            dma((ny, CHUNKS)),
            dma((ny, CHUNKS)),
            dma((ny, CHUNKS)),
            dma,
            dma,
            dma((nx,)),
            dma((nx,)),
            pltpu.VMEM((FEAT, tok_dev), BF16),
            pltpu.VMEM((2, tok_dev), F32),
            pltpu.VMEM((hid, model), F32),
            pltpu.VMEM((hid, model), F32),
            pltpu.VMEM((hid, model), F32),
            dma((5,)),
        ],
        compiler_params=pltpu.CompilerParams(
            collective_id=0, has_side_effects=True, vmem_limit_bytes=62 * 1024 * 1024
        ),
        name="experts_backward",
    )(
        tokens,
        cotangent,
        routes.T,
        route_weight.T,
        w_gate[0].T,
        w_up[0].T,
        w_down[0],
    )
    g_tok, g_rw, g_gate, g_up, g_down = pl.pallas_call(
        store,
        out_shape=tuple(jax.ShapeDtypeStruct(o.shape, o.dtype) for o in outs),
        in_specs=[hbm] * 5,
        out_specs=[hbm] * 5,
        scratch_shapes=[pltpu.VMEM(o.shape, o.dtype) for o in outs] + [dma((2, 5))],
        compiler_params=pltpu.CompilerParams(vmem_limit_bytes=62 * 1024 * 1024),
        name="store",
    )(*outs)
    return g_tok.T, g_rw.T, g_gate.T[None], g_up.T[None], g_down[None]


def solution(mesh):
    nz = mesh.shape["ep"] // 2
    nx = 4 if mesh.shape["tp"] >= 16 else 2
    ny = mesh.shape["tp"] // nx
    return jax.shard_map(
        functools.partial(on_device, nz, ny, nx),
        mesh=mesh,
        in_specs=(
            P("ep", None),
            P("ep", None),
            P("ep", None),
            P("ep", None),
            P("ep", None, "tp"),
            P("ep", None, "tp"),
            P("ep", "tp", None),
        ),
        out_specs=(
            P("ep", "tp"),
            P("ep", None),
            P("ep", None, "tp"),
            P("ep", None, "tp"),
            P("ep", "tp", None),
        ),
        check_vma=False,
    )
```

time: 103 us -> 85 us (0.83)
  Pallas kernels: 93.3 us -> 84.1 us
  local copies, waits for them, and re-layouts: 8.75 us -> 0 us
    pallas_call x1, Pallas kernels: 93.3 us -> 82.1 us  [on_device(): pl.pallas_call(functools.partial(kernel, nz, ny, nx, cap), out_shape=(jax...]
    unnamed x19 -> x0, local copies, waits for them, and re-layouts: 8.75 us -> none
    pallas_call x0 -> x1, Pallas kernels: none -> 1.93 us  [on_device(): pl.pallas_call(store, out_shape=tuple((jax.ShapeDtypeStruct(o.shape, o.dt...]
where the time goes in v2:
time: 85 us; the launch traced here: 84.7 us
  Pallas kernels  84.1 us (99%)
    pallas_call x1, Pallas kernels, on_device(): pl.pallas_call(functools.partial(kernel, nz, ny, nx, cap), out_shape=(jax...  82.1 us
    pallas_call x1, Pallas kernels, on_device(): pl.pallas_call(store, out_shape=tuple((jax.ShapeDtypeStruct(o.shape, o.dt...  1.93 us

profile of v2, /device:TPU:1, one launch (start us, length us, event | category | flops | bytes accessed | tf_op | source)
XLA Modules:
  0.0 84.7 jit_solution(9838326181328358492)
XLA Ops:
  0.6 82.1 %experts_backward.1 = (bf16[64,128]{1,0:T(8,128)(2,1)}, f32[2,128]{1,0:T(2,128)}, f32[32,2048]{1,0:T(8,128)}, f32[32,2048]{1,0:T(8,128)}, f32[32,2048]{1,0:T(8,128)}) custom-call(bf16[128,2048]{1,0:T(8,128)(2,1)} %tokens.1, bf16[128,2048]{1,0:T(8,128)(2,1)} %cotangent.1, s32[2,128]{1,0:T(2,128)} %bitcast.21, f32[2,128]{1,0:T(2,128)} %bitcast.22, ...), custom_call_target="tpu_custom_call" | custom-call | tf_op jit(solution)/shard_map/experts_backward/pallas_call | solution.py:410
  82.8 1.9 %store.1 = (bf16[64,128]{1,0:T(8,128)(2,1)}, f32[2,128]{1,0:T(2,128)}, f32[32,2048]{1,0:T(8,128)}, f32[32,2048]{1,0:T(8,128)}, f32[32,2048]{1,0:T(8,128)}) custom-call(bf16[64,128]{1,0:T(8,128)(2,1)} %get-tuple-element.15.refs_0_, f32[2,128]{1,0:T(2,128)} %get-tuple-element.16.refs_1_, f32[32,2048]{1,0:T(8,128)} %get-tuple-element.17.refs_2_, ...), custom_call_target="tpu_custom_call" | custom-call | tf_op jit(solution)/shard_map/store/pallas_call | solution.py:486

commit v3 on v2

--- a/solution.py
+++ b/solution.py
@@ -189,7 +189,8 @@
     steps = ny // 2
     per = count // CHUNKS
     pack = per // 2
-    order = [0, 1, 3, 2]
+    order = [2, 1, 3, 0]
+    copies_wide = LANES // per
     lane_c = lax.broadcasted_iota(jnp.int32, (per, LANES), 1)
     lane_p = lax.broadcasted_iota(jnp.int32, (pack, LANES), 1)
     pick = (lax.broadcasted_iota(jnp.int32, (16, nx * LANES), 1) % LANES == 3 * HID).astype(F32).astype(BF16)
@@ -206,33 +207,44 @@
     def chunk_rows(i):
         return pl.ds(pl.multiple_of(chunk_of(i) * per, per), per)
 
-    def ring(way, step, i, owner):
+    def toward(way, hops):
+        return (y + hops) % ny if way == 0 else (y + ny - hops) % ny
+
+    def reach(way, hops, i):
+        step, owner = (hops, y) if hops <= 2 else (hops - 2, toward(1 - way, 2))
         block = rows.at[chunk_rows(i), col(owner)]
-        to = y_peer(1) if way == 0 else y_peer(ny - 1)
         return remote(
-            block, block, ag_ssem.at[way, step - 1, i], ag_rsem.at[way, step - 1, i], ep, to
+            block, block, ag_ssem.at[way, hops - 1, i], ag_rsem.at[way, hops - 1, i],
+            ep, toward(way, step) * nx + x,
         )
 
-    def owner_of(way, hops):
-        return (y + ny - hops) % ny if way == 0 else (y + hops) % ny
-
-    def travels(way, step, i):
-        return step < steps or (i < CHUNKS // 2) == (way == 0)
-
-    def gather(i, step):
-        if step == 1:
-            if order[i] == 0:
-                arrived(rows.at[pl.ds(0, per - cap), col(y)], z_recv.at[chunk_of(i)])
-            else:
-                arrived(rows.at[chunk_rows(i), col(y)], z_recv.at[chunk_of(i)])
+    def reached(way, hops, i):
+        arrived(rows.at[chunk_rows(i), col(toward(1 - way, hops))], ag_rsem.at[way, hops - 1, i])
+
+    def travels(way, hops, i):
+        return hops < steps or (i < CHUNKS // 2) == (way == 0)
+
+    def spread_near(i):
+        if order[i] == 0:
+            arrived(rows.at[pl.ds(0, per - cap), col(y)], z_recv.at[chunk_of(i)])
+        else:
+            arrived(rows.at[chunk_rows(i), col(y)], z_recv.at[chunk_of(i)])
+        for hops in (2, 1):
+            for way in (0, 1):
+                launch(reach(way, hops, i))
+
+    def spread_far(i):
         for way in (0, 1):
-            if step > 1 and travels(way, step - 1, i):
-                ring(way, step - 1, i, owner_of(way, step - 1)).wait_recv()
-            if step <= steps and travels(way, step, i):
-                launch(ring(way, step, i, owner_of(way, step - 1)))
+            reached(way, 2, i)
+            for hops in (4, 3):
+                if travels(way, hops, i):
+                    launch(reach(way, hops, i))
 
     def partial(i):
-        gather(i, steps + 1)
+        for hops in (1, 3, 4):
+            for way in (0, 1):
+                if travels(way, hops, i):
+                    reached(way, hops, i)
         if i == 0:
             for d in range(1, nx):
                 arrived(w_all.at[w_place((x + nx - d) % nx), :], w_rsem.at[d])
@@ -281,7 +293,7 @@
             tile = slice(j * LANES, (j + 1) * LANES)
             right = pltpu.roll(whole[pack:per, tile], FEAT, 1)
             piece[i, :, tile] = jnp.where(lane_p < FEAT, whole[0:pack, tile], right).astype(BF16)
-        rw_row[i] = dot(pick, value, 1, 1)[0:1, :]
+        rw_row[i] = jnp.concatenate([dot(pick, value, 1, 1)[0:1, :]] * copies_wide, axis=1)
         for d in y_order:
             launch(
                 remote(
@@ -304,10 +316,8 @@
             arrived(rw_got.at[d, i], rw_rsem.at[d, i])
             total = total + piece_got[d, i].astype(F32)
             total_rw = total_rw + rw_got[d, i]
-        spread_rw = jnp.broadcast_to(total_rw, (per, per)).T
+        spread_rw = jnp.broadcast_to(total_rw, (LANES, LANES)).T[0:per, :]
         both_ = jnp.concatenate([total, pltpu.roll(total, FEAT, 1)], axis=0)
-        if per < LANES:
-            spread_rw = jnp.broadcast_to(spread_rw[:, 0:1], (per, LANES))
         back[chunk_rows(i), :] = jnp.where(lane_c < FEAT, both_, spread_rw).astype(BF16)
         base = chunk_of(i) * group
         if order[i] == 0:
@@ -316,19 +326,22 @@
             send_back(base + (ep + j) % group)
 
     x_order = list(range(1, nx))
-    stages = [functools.partial(gather, step=s) for s in range(1, steps + 1)]
-    stages += [partial, activate, token_part, summed]
-    for wave in range(len(stages) + CHUNKS - 1):
-        if wave == len(stages) + CHUNKS - 2:
+    stages = [spread_near, spread_far, partial, activate, token_part, summed]
+    after = [0, 4, 8, 13, 18, 26]
+    turns = sorted(
+        (after[k] + 3 * i, k, i) for k in range(len(stages)) for i in range(CHUNKS)
+    )
+    for _, k, i in turns:
+        if (k, i) == (len(stages) - 1, CHUNKS - 1):
             grads = dot(hidden[...], rows[...], 0, 0)
             g_lane = lax.broadcasted_iota(jnp.int32, (HID, ny * LANES), 1) % LANES
-            for k in range(nx):
-                at = k * LANES
+            for n in range(nx):
+                at = n * LANES
                 gate_down = jnp.where(
                     g_lane < FEAT, grads[at : at + HID, :], grads[at + 2 * HID : at + 3 * HID, :]
                 )
-                grad_send[k, 0:HID, :] = gate_down.astype(BF16)
-                grad_send[k, HID : 2 * HID, :] = grads[at + HID : at + 2 * HID, :].astype(BF16)
+                grad_send[n, 0:HID, :] = gate_down.astype(BF16)
+                grad_send[n, HID : 2 * HID, :] = grads[at + HID : at + 2 * HID, :].astype(BF16)
             for d in range(1, nx):
                 launch(
                     remote(
@@ -337,9 +350,7 @@
                     )
                 )
             grad_got[x] = grad_send[x]
-        for k, stage in enumerate(stages):
-            if 0 <= wave - k < CHUNKS:
-                stage(wave - k)
+        stages[k](i)
 
     for d in range(1, nx):
         arrived(grad_got.at[(x + nx - d) % nx], g_rsem.at[d])
@@ -438,8 +449,8 @@
             pltpu.VMEM((count, wide_x), BF16),
             pltpu.VMEM((CHUNKS, per // 2, wide_y), BF16),
             pltpu.VMEM((ny, CHUNKS, per // 2, LANES), BF16),
-            pltpu.VMEM((CHUNKS, 1, per), F32),
-            pltpu.VMEM((ny, CHUNKS, 1, per), F32),
+            pltpu.VMEM((CHUNKS, 1, LANES), F32),
+            pltpu.VMEM((ny, CHUNKS, 1, LANES), F32),
             pltpu.VMEM((count, LANES), BF16),
             pltpu.VMEM((count, LANES), BF16),
             pltpu.VMEM((nx, 2 * HID, wide_y), BF16),

time: 85 us -> 76.9 us (0.905)
  Pallas kernels: 84.1 us -> 76 us
    pallas_call x1, Pallas kernels: 82.1 us -> 74.1 us  [on_device(): pl.pallas_call(functools.partial(kernel, nz, ny, nx, cap), out_shape=(jax...]
where the time goes in v3:
time: 76.9 us; the launch traced here: 76.7 us
  Pallas kernels  76 us (99%)
    pallas_call x1, Pallas kernels, on_device(): pl.pallas_call(functools.partial(kernel, nz, ny, nx, cap), out_shape=(jax...  74.1 us
    pallas_call x1, Pallas kernels, on_device(): pl.pallas_call(store, out_shape=tuple((jax.ShapeDtypeStruct(o.shape, o.dt...  1.93 us

profile of v3, /device:TPU:1, one launch (start us, length us, event | category | flops | bytes accessed | tf_op | source)
XLA Modules:
  0.0 76.7 jit_solution(15390535213403400240)
XLA Ops:
  0.6 74.1 %experts_backward.1 = (bf16[64,128]{1,0:T(8,128)(2,1)}, f32[2,128]{1,0:T(2,128)}, f32[32,2048]{1,0:T(8,128)}, f32[32,2048]{1,0:T(8,128)}, f32[32,2048]{1,0:T(8,128)}) custom-call(bf16[128,2048]{1,0:T(8,128)(2,1)} %tokens.1, bf16[128,2048]{1,0:T(8,128)(2,1)} %cotangent.1, s32[2,128]{1,0:T(2,128)} %bitcast.21, f32[2,128]{1,0:T(2,128)} %bitcast.22, ...), custom_call_target="tpu_custom_call" | custom-call | tf_op jit(solution)/shard_map/experts_backward/pallas_call | solution.py:421
  74.7 1.9 %store.1 = (bf16[64,128]{1,0:T(8,128)(2,1)}, f32[2,128]{1,0:T(2,128)}, f32[32,2048]{1,0:T(8,128)}, f32[32,2048]{1,0:T(8,128)}, f32[32,2048]{1,0:T(8,128)}) custom-call(bf16[64,128]{1,0:T(8,128)(2,1)} %get-tuple-element.15.refs_0_, f32[2,128]{1,0:T(2,128)} %get-tuple-element.16.refs_1_, f32[32,2048]{1,0:T(8,128)} %get-tuple-element.17.refs_2_, ...), custom_call_target="tpu_custom_call" | custom-call | tf_op jit(solution)/shard_map/store/pallas_call | solution.py:497

commit v4 on v3

--- a/solution.py
+++ b/solution.py
@@ -70,23 +70,6 @@
     def slot(e):
         return pl.ds(pl.multiple_of(e * cap, cap), cap)
 
-    barrier = pltpu.get_barrier_semaphore()
-
-    def greet(to_ep, to_tp):
-        pl.semaphore_signal(barrier, inc=1, device_id=(to_ep, to_tp), device_id_type=MESH)
-
-    def greet_ep(i, carry):
-        greet(ep_peer(i, 0), tp)
-        greet(ep_peer(i, 1), tp)
-        return carry
-
-    lax.fori_loop(0, nz - 1, greet_ep, 0)
-    greet(ep_peer(nz - 1, 1), tp)
-    for d in range(1, nx):
-        greet(ep, x_peer(d))
-    for d in range(1, ny):
-        greet(ep, y_peer(d))
-
     pair = col(tp // 2)
     loads = [
         pltpu.make_async_copy(tokens.at[:, pair], tok_in, in_sem.at[0]),
@@ -99,6 +82,23 @@
     ]
     for load in loads[5:] + loads[:5]:
         load.start()
+    barrier = pltpu.get_barrier_semaphore()
+
+    def greet(to_ep, to_tp):
+        pl.semaphore_signal(barrier, inc=1, device_id=(to_ep, to_tp), device_id_type=MESH)
+
+    def greet_ep(i, carry):
+        greet(ep_peer(i, 0), tp)
+        greet(ep_peer(i, 1), tp)
+        return carry
+
+    lax.fori_loop(0, nz - 1, greet_ep, 0)
+    greet(ep_peer(nz - 1, 1), tp)
+    for d in range(1, nx):
+        greet(ep, x_peer(d))
+    for d in range(1, ny):
+        greet(ep, y_peer(d))
+
     loads[5].wait()
     loads[6].wait()
 
@@ -196,6 +196,7 @@
     pick = (lax.broadcasted_iota(jnp.int32, (16, nx * LANES), 1) % LANES == 3 * HID).astype(F32).astype(BF16)
     y_order = [ny // 2 + (k + 1) // 2 * (1 if k % 2 == 0 else -1) for k in range(ny - 1)]
     copies = []
+    x_order = sorted(range(1, nx), key=lambda d: -min(d, nx - d))
 
     def launch(copy):
         copy.start()
@@ -248,8 +249,13 @@
         if i == 0:
             for d in range(1, nx):
                 arrived(w_all.at[w_place((x + nx - d) % nx), :], w_rsem.at[d])
-        part_send[i] = dot(rows[chunk_rows(i), :], w_all[...], 1, 1).astype(BF16)
-        for d in x_order:
+        block = rows[chunk_rows(i), :]
+        for d in x_order + [0]:
+            to = (x + d) % nx
+            w_to = w_all[pl.ds(pl.multiple_of(to * LANES, LANES), LANES), :]
+            part_send[i, :, col(to)] = dot(block, w_to, 1, 1).astype(BF16)
+            if d == 0:
+                break
             launch(
                 remote(
                     part_send.at[i, :, col((x + d) % nx)], part_got.at[d, i],
@@ -325,11 +331,11 @@
         for j in range(1 if order[i] == 0 else 0, group):
             send_back(base + (ep + j) % group)
 
-    x_order = list(range(1, nx))
     stages = [spread_near, spread_far, partial, activate, token_part, summed]
     after = [0, 4, 8, 13, 18, 26]
+    apart = [2.5, 3, 3.5, 3.5, 3.5, 3.5]
     turns = sorted(
-        (after[k] + 3 * i, k, i) for k in range(len(stages)) for i in range(CHUNKS)
+        (after[k] + apart[k] * i, k, i) for k in range(len(stages)) for i in range(CHUNKS)
     )
     for _, k, i in turns:
         if (k, i) == (len(stages) - 1, CHUNKS - 1):

time: 76.9 us -> 77 us (level)
  no operation moved by 1% of the time
where the time goes in v4:
time: 77 us; the launch traced here: 76.8 us
  Pallas kernels  76.2 us (99%)
    pallas_call x1, Pallas kernels, on_device(): pl.pallas_call(functools.partial(kernel, nz, ny, nx, cap), out_shape=(jax...  74.2 us
    pallas_call x1, Pallas kernels, on_device(): pl.pallas_call(store, out_shape=tuple((jax.ShapeDtypeStruct(o.shape, o.dt...  1.93 us

profile of v4, /device:TPU:1, one launch (start us, length us, event | category | flops | bytes accessed | tf_op | source)
XLA Modules:
  0.0 76.8 jit_solution(2508388949446504072)
XLA Ops:
  0.6 74.2 %experts_backward.1 = (bf16[64,128]{1,0:T(8,128)(2,1)}, f32[2,128]{1,0:T(2,128)}, f32[32,2048]{1,0:T(8,128)}, f32[32,2048]{1,0:T(8,128)}, f32[32,2048]{1,0:T(8,128)}) custom-call(bf16[128,2048]{1,0:T(8,128)(2,1)} %tokens.1, bf16[128,2048]{1,0:T(8,128)(2,1)} %cotangent.1, s32[2,128]{1,0:T(2,128)} %bitcast.21, f32[2,128]{1,0:T(2,128)} %bitcast.22, ...), custom_call_target="tpu_custom_call" | custom-call | tf_op jit(solution)/shard_map/experts_backward/pallas_call | solution.py:427
  74.9 1.9 %store.1 = (bf16[64,128]{1,0:T(8,128)(2,1)}, f32[2,128]{1,0:T(2,128)}, f32[32,2048]{1,0:T(8,128)}, f32[32,2048]{1,0:T(8,128)}, f32[32,2048]{1,0:T(8,128)}) custom-call(bf16[64,128]{1,0:T(8,128)(2,1)} %get-tuple-element.15.refs_0_, f32[2,128]{1,0:T(2,128)} %get-tuple-element.16.refs_1_, f32[32,2048]{1,0:T(8,128)} %get-tuple-element.17.refs_2_, ...), custom_call_target="tpu_custom_call" | custom-call | tf_op jit(solution)/shard_map/store/pallas_call | solution.py:503
